TPU v7x, 32 devices: a whole 2x2x4 slice. The times are simulated.
32 devices in a mesh: ep: 16 (over z, y, x), tp: 2 (over core).
Axes of the slice: x: 2, y: 2, z: 4, core: 2. Of those that a mesh axis runs over, the one named last changes fastest.
Arguments:
- tokens: bfloat16 [768, 2048], P('ep', 'tp'), may hold values from -12 to 12
- conv_state: bfloat16 [768, 3, 1024], P('ep', None, 'tp'), may hold values from -6 to 6
- hidden_state: float32 [768, 1024], P('ep', 'tp'), may hold values from -6 to 6
- mixer_gain: float32 [2048], replicated, may hold values from 0.1 to 1.9
- branch_weight: bfloat16 [2048, 1024], P(None, 'tp'), may hold values from -0.125 to 0.125
- gelu_weight: bfloat16 [2048, 1024], P(None, 'tp'), may hold values from -0.125 to 0.125
- conv_kernel: float32 [4, 1024], P(None, 'tp'), may hold values from -3 to 3
- recur_blocks: bfloat16 [16, 64, 64], P('tp'), may hold values from -0.75 to 0.75
- input_blocks: bfloat16 [16, 64, 64], P('tp'), may hold values from -0.75 to 0.75
- decay_rate: float32 [1024], P('tp'), may hold values from 0.002 to 0.1
- output_weight: bfloat16 [1024, 2048], P(None, 'tp'), may hold values from -0.1875 to 0.1875
- expert_gain: float32 [2048], replicated, may hold values from 0.1 to 1.9
- expert_ids: int32 [768, 2], P('ep'), may hold values from 0 to 15, as said below
- group_prob: float32 [768], P('ep'), may hold values from 0.25 to 1
- expert_logit: float32 [768, 2], P('ep'), may hold values from -4 to 4
- expert_gate: bfloat16 [16, 2048, 512], P('ep', None, 'tp'), may hold values from -0.125 to 0.125
- expert_up: bfloat16 [16, 2048, 512], P('ep', None, 'tp'), may hold values from -0.125 to 0.125
- expert_down: bfloat16 [16, 512, 2048], P('ep', 'tp'), may hold values from -0.25 to 0.25
Outputs:
- layer_out: bfloat16 [768, 2048], P('ep', 'tp')
- new_hidden: float32 [768, 1024], P('ep', 'tp')
Inputs may be any that keep to these rules, and one draw needn't show every extreme that they name: `expert_ids`: the two experts of a row are different and lie in one group of 4 consecutive experts. Within the rows of one index of ep no expert is named more than 6 times, and one expert is named exactly 6 times by the rows of every index of ep.
All inputs are finite; a program needn't handle non-finite values.
Results may differ from a plain program's by a relative error of at most 0.012.
Values may be sent and summed in bfloat16 or wider, within the bound.
A program may use at most 64 MiB of HBM per device.

v0:
```python
import jax
import jax.numpy as jnp
from jax import lax
from jax.sharding import PartitionSpec as P

EPSILON = 1e-06
RATE_SCALE = 8.0


def normalize(values, gain_row):
    squares = jnp.mean(values * values, axis=-1, keepdims=True)
    return values * lax.rsqrt(squares + EPSILON) * gain_row


def local(
    tokens,
    conv_state,
    hidden_state,
    mixer_gain,
    branch_weight,
    gelu_weight,
    conv_kernel,
    recur_blocks,
    input_blocks,
    decay_rate,
    output_weight,
    expert_gain,
    expert_ids,
    group_prob,
    expert_logit,
    expert_gate,
    expert_up,
    expert_down,
):
    whole_tokens = lax.all_gather(tokens, "tp", axis=1, tiled=True)
    normed = normalize(whole_tokens.astype(jnp.float32), mixer_gain).astype(jnp.bfloat16)
    branch = jnp.dot(normed, branch_weight, preferred_element_type=jnp.float32).astype(jnp.bfloat16)
    gelu_input = jnp.dot(normed, gelu_weight, preferred_element_type=jnp.float32).astype(
        jnp.bfloat16
    )
    window = jnp.concatenate([conv_state, branch[:, None, :]], axis=1).astype(jnp.float32)
    convolved = jnp.sum(window * conv_kernel[None], axis=1).astype(jnp.bfloat16)
    sequences, channels = convolved.shape
    blocks, block_size = (recur_blocks.shape[0], recur_blocks.shape[1])
    grouped = convolved.reshape(sequences, blocks, block_size)
    recur_pre = jnp.einsum(
        "tnc,ncd->tnd", grouped, recur_blocks, preferred_element_type=jnp.float32
    ).reshape(sequences, channels)
    input_pre = jnp.einsum(
        "tnc,ncd->tnd", grouped, input_blocks, preferred_element_type=jnp.float32
    ).reshape(sequences, channels)
    recur_gate = jax.nn.sigmoid(recur_pre)
    input_gate = jax.nn.sigmoid(input_pre)
    log_decay = -RATE_SCALE * recur_gate * decay_rate
    new_hidden = jnp.exp(log_decay) * hidden_state + jnp.sqrt(-jnp.expm1(2.0 * log_decay)) * (
        input_gate * convolved.astype(jnp.float32)
    )
    mixed_rows = (
        new_hidden * jax.nn.gelu(gelu_input.astype(jnp.float32), approximate=True)
    ).astype(jnp.bfloat16)
    mixed_whole = lax.all_gather(mixed_rows, "tp", axis=1, tiled=True)
    residual = (
        tokens.astype(jnp.float32)
        + jnp.dot(mixed_whole, output_weight, preferred_element_type=jnp.float32)
    ).astype(jnp.bfloat16)
    experts = lax.axis_size("ep")
    top_count = expert_ids.shape[1]
    capacity = 2 * max(1, sequences // experts)
    flat_ids = expert_ids.reshape(-1)
    onehot_ids = (flat_ids[:, None] == jnp.arange(experts, dtype=jnp.int32)[None, :]).astype(
        jnp.int32
    )
    earlier = jnp.cumsum(onehot_ids, axis=0) - onehot_ids
    ranking = jnp.sum(earlier * onehot_ids, axis=1)
    slot_index = flat_ids * capacity + ranking
    placing = (
        jnp.arange(experts * capacity, dtype=jnp.int32)[:, None] == slot_index[None, :]
    ).astype(jnp.float32)
    placing = jnp.sum(placing.reshape(experts * capacity, sequences, top_count), axis=2).astype(
        jnp.bfloat16
    )
    values = residual.astype(jnp.float32)
    half_width = values.shape[1]
    square_total = lax.psum(jnp.sum(values * values, axis=1), "tp")
    gain_part = lax.dynamic_slice_in_dim(
        expert_gain, lax.axis_index("tp") * half_width, half_width, 0
    )
    scaling = lax.rsqrt(square_total / (half_width * lax.axis_size("tp")) + EPSILON)
    moe_input = (values * scaling[:, None] * gain_part[None, :]).astype(jnp.bfloat16)
    outgoing = jnp.dot(placing, moe_input, preferred_element_type=jnp.float32).astype(jnp.bfloat16)
    outgoing = outgoing.reshape(experts, capacity, half_width)
    received = lax.all_gather(
        lax.all_to_all(outgoing, "ep", split_axis=0, concat_axis=0, tiled=True),
        "tp",
        axis=2,
        tiled=True,
    )
    sources, slot_count, features = received.shape
    flat_rows = received.reshape(sources * slot_count, features)
    gate_part = jnp.dot(flat_rows, expert_gate[0], preferred_element_type=jnp.float32)
    upper_part = jnp.dot(flat_rows, expert_up[0], preferred_element_type=jnp.float32)
    hidden_units = (jax.nn.silu(gate_part) * upper_part).astype(jnp.bfloat16)
    partial_value = jnp.dot(
        hidden_units, expert_down[0], preferred_element_type=jnp.float32
    ).reshape(sources, slot_count, features)
    summed = lax.psum_scatter(
        partial_value.astype(jnp.bfloat16), "tp", scatter_dimension=2, tiled=True
    )
    returned = lax.all_to_all(summed, "ep", split_axis=0, concat_axis=0, tiled=True)
    out_width = returned.shape[2]
    picked = jnp.take(returned.reshape(experts * capacity, out_width), slot_index, axis=0).reshape(
        sequences, top_count, out_width
    )
    logit_exp = jnp.exp(expert_logit)
    weights = group_prob[:, None] * logit_exp / jnp.sum(logit_exp, axis=1, keepdims=True)
    layer_out = (
        residual.astype(jnp.float32)
        + jnp.sum(weights[:, :, None] * picked.astype(jnp.float32), axis=1)
    ).astype(jnp.bfloat16)
    return (layer_out, new_hidden)


def solution(mesh):
    return jax.shard_map(
        local,
        mesh=mesh,
        in_specs=(
            P("ep", "tp"),
            P("ep", None, "tp"),
            P("ep", "tp"),
            P(),
            P(None, "tp"),
            P(None, "tp"),
            P(None, "tp"),
            P("tp", None, None),
            P("tp", None, None),
            P("tp"),
            P(None, "tp"),
            P(),
            P("ep", None),
            P("ep"),
            P("ep", None),
            P("ep", None, "tp"),
            P("ep", None, "tp"),
            P("ep", "tp", None),
        ),
        out_specs=(P("ep", "tp"), P("ep", "tp")),
        check_vma=False,
    )
```

profile of v0, /device:TPU:0, one launch (start us, length us, event | category | flops | bytes accessed | tf_op | source)
XLA Modules:
  0.0 81.5 jit_solution(5412062372316779908)
XLA Ops:
  7.2 0.0 copy-start
  7.2 0.0 copy-start.3
  7.2 0.0 copy-start.7
  7.2 0.0 copy-start.12
  7.2 0.0 reduce-scatter.2.cloned.1.call-start
  7.3 2.4 %all_gather.9 = bf16[48,2048]{1,0:T(8,128)(2,1)S(1)} all-gather(bf16[48,1024]{1,0:T(8,128)(2,1)} %param.18), channel_id=1, replica_groups=mesh['ep'=16,'tp'=2] {'tp'}, dimensions={1}, use_global_device_ids=true | all-gather | bytes 294912 | tf_op jit(solution)/shard_map/all_gather | solution.py:35
  9.7 0.1 fusion.17
  9.8 2.2 %fusion.12 = bf16[48,1,512]{2,0,1:T(8,128)(2,1)S(1)} fusion(bf16[2048,512]{1,0:T(8,128)(2,1)} %param.22, bf16[48,2048]{1,0:T(8,128)(2,1)S(1)} %all_gather.9, f32[2048]{0:T(1024)} %param.21, f32[48]{0:T(128)S(1)} %add_rsqrt_fusion.1), kind=kOutput, calls=%fused_computation.21 | convolution fusion | flops 101081088 | bytes 2351296 | tf_op jit(solution)/shard_map/dot_general | solution.py:37
  12.0 0.0 copy-done.3
  12.0 0.0 copy-done.7
  12.0 0.0 copy-start.9
  12.0 0.0 copy-start.4
  12.1 0.0 copy-start.5
  12.1 0.1 convert_element_type.75
  12.2 0.0 copy-done.12
  12.2 0.2 fusion.7
  12.5 0.1 copy.55
  12.5 0.1 div.37
  12.6 0.2 fusion.3
  12.8 0.0 copy-start.1
  12.9 0.1 copy.57
  12.9 0.1 div.39
  13.1 0.1 multiply_add_fusion
  13.2 0.0 copy-done.5
  13.2 0.0 copy-start.2
  13.2 0.0 copy-start.6
  13.2 2.2 %fusion.28 = bf16[48,512]{1,0:T(8,128)(2,1)S(1)} fusion(f32[48,512]{1,0:T(8,128)S(1)} %multiply_add_fusion, bf16[2048,512]{1,0:T(8,128)(2,1)} %param.23, bf16[48,2048]{1,0:T(8,128)(2,1)S(1)} %all_gather.9, f32[2048]{0:T(1024)S(1)} %copy-done.5, f32[48]{0:T(128)S(1)} %add_rsqrt_fusion.1), kind=kOutput, calls=%fused_computation.46 | convolution fusion | flops 101351424 | bytes 2449600 | tf_op jit(solution)/shard_map/dot_general | solution.py:38
  15.4 0.0 copy-start.8
  15.4 1.9 %all_gather.10 = bf16[48,1024]{1,0:T(8,128)(2,1)S(1)} all-gather(bf16[48,512]{1,0:T(8,128)(2,1)S(1)} %fusion.28), channel_id=1, replica_groups=mesh['ep'=16,'tp'=2] {'tp'}, dimensions={1}, use_global_device_ids=true | all-gather | bytes 147456 | tf_op jit(solution)/shard_map/all_gather | solution.py:61
  17.3 0.6 multiply_reduce_fusion.2
  17.9 0.0 copy-done.2
  17.9 2.5 %psum.7 = f32[48]{0:T(128)S(1)} all-reduce(f32[48]{0:T(128)S(1)} %get-tuple-element.4), channel_id=1, replica_groups=mesh['ep'=16,'tp'=2] {'tp'}, use_global_device_ids=true, to_apply=%region_7.8 | all-reduce | flops 48 | bytes 384 | tf_op jit(solution)/shard_map/psum | solution.py:84
  20.4 0.1 copy.59
  20.5 0.1 reshape.111
  20.6 0.1 fusion.36
  20.7 0.1 reduce_window_sum.11
  20.8 0.2 select_reduce_fusion
  21.0 0.1 reduce_sum.71
  21.1 0.1 copy.60
  21.2 0.1 convert_reduce_fusion
  21.3 0.3 convolution_convert_fusion.1
  21.6 0.1 reshape.112
  21.7 18.2 %all_to_all.10 = bf16[16,6,1024]{2,1,0:T(8,128)(2,1)S(1)} all-to-all(bf16[16,6,1024]{2,1,0:T(8,128)(2,1)S(1)} %reshape.112), channel_id=1, replica_groups=mesh['ep'=16,'tp'=2] {'ep'}, dimensions={0} | all-to-all | bytes 393216 | tf_op jit(solution)/shard_map/all_to_all | solution.py:93
  39.9 2.2 %all_gather.11 = bf16[16,6,2048]{2,1,0:T(8,128)(2,1)S(1)} all-gather(bf16[16,6,1024]{2,1,0:T(8,128)(2,1)S(1)} %all_to_all.10), channel_id=1, replica_groups=mesh['ep'=16,'tp'=2] {'tp'}, dimensions={2}, use_global_device_ids=true | all-gather | bytes 589824 | tf_op jit(solution)/shard_map/all_gather | solution.py:92
  42.0 0.1 reshape.113
  42.2 1.5 %fusion.15 = f32[96,256]{1,0:T(8,128)S(1)} fusion(bf16[96,2048]{1,0:T(8,128)(2,1)S(1)} %reshape.113, bf16[1,2048,256]{2,1,0:T(8,128)(2,1)} %param.33), kind=kOutput, calls=%fused_computation.24 | convolution fusion | flops 100663296 | bytes 1540096 | tf_op jit(solution)/shard_map/dot_general | solution.py:100
  43.7 0.0 copy-start.10
  43.7 0.0 copy-start.11
  43.7 1.5 %fusion.10 = bf16[96,256]{1,0:T(8,128)(2,1)S(1)} fusion(bf16[96,2048]{1,0:T(8,128)(2,1)S(1)} %reshape.113, bf16[1,2048,256]{2,1,0:T(8,128)(2,1)} %param.34, f32[96,256]{1,0:T(8,128)S(1)} %fusion.15), kind=kOutput, calls=%fused_computation.17 | convolution fusion | flops 100810752 | bytes 1589248 | tf_op jit(solution)/shard_map/dot_general | solution.py:101
  45.3 2.3 %convolution_convert_fusion = bf16[16,6,2048]{2,0,1:T(8,128)(2,1)} fusion(bf16[1,256,2048]{2,1,0:T(8,128)(2,1)} %param.35, bf16[16,6,256]{2,1,0:T(8,128)(2,1)S(1)} %dot_general.37), kind=kOutput, calls=%fused_computation.1 | convolution fusion | flops 100859904 | bytes 1490944 | tf_op jit(solution)/shard_map/dot_general | solution.py:103
  47.6 0.0 reduce-scatter.2.cloned.1.call-update
  47.7 5.8 %reduce-scatter.2.cloned.1.call-done = bf16[16,6,1024]{2,0,1:T(8,128)(2,1)} async-done(((bf16[16,6,2048]{2,0,1:T(8,128)(2,1)}), bf16[16,6,1024]{2,0,1:T(8,128)(2,1)}) %reduce-scatter.2.cloned.1.call-update) | async-done | bytes 196624 | tf_op jit(solution)/shard_map/reduce_scatter | solution.py:106
  53.5 1.7 %copy.63 = bf16[16,6,1024]{2,1,0:T(8,128)(2,1)} copy(bf16[16,6,1024]{2,0,1:T(8,128)(2,1)} %reduce-scatter.2.cloned.1.call-done) | data formatting | bytes 393216 | tf_op jit(solution)/shard_map/reduce_scatter | solution.py:106
  55.2 6.7 %all-to-all-start.1 = ((bf16[16,6,1024]{2,1,0:T(8,128)(2,1)}), bf16[16,6,1024]{2,1,0:T(8,128)(2,1)S(1)}, u32[]{:S(2)}, u32[]{:S(2)}) async-start(bf16[16,6,1024]{2,1,0:T(8,128)(2,1)} %copy.63), calls=%async_computation.2 | async-start | bytes 524288 | tf_op jit(solution)/shard_map/all_to_all | solution.py:109
  62.0 0.1 copy.64
  62.1 0.1 mul.189
  62.2 0.1 copy.61
  62.3 0.1 copy.58
  62.4 9.9 %all-to-all-done.1 = bf16[16,6,1024]{2,1,0:T(8,128)(2,1)S(1)} async-done(((bf16[16,6,1024]{2,1,0:T(8,128)(2,1)}), bf16[16,6,1024]{2,1,0:T(8,128)(2,1)S(1)}, u32[]{:S(2)}, u32[]{:S(2)}) %all-to-all-start.1) | async-done | bytes 196640 | tf_op jit(solution)/shard_map/all_to_all | solution.py:109
  72.4 0.1 reshape.114
  72.4 0.8 gather_fusion
  73.2 0.1 gather.7
  73.3 0.7 multiply_reduce_fusion
  74.0 0.7 add_convert_fusion
  (22 shorter events, 0.2 us)
Async XLA Ops:
  7.2 10.1 %copy-start = (bf16[1024,1024]{1,0:T(8,128)(2,1)S(1)}, bf16[1024,1024]{1,0:T(8,128)(2,1)}, u32[]{:S(2)}) copy-start(bf16[1024,1024]{1,0:T(8,128)(2,1)} %param.28) | copy-start | bytes 6291460
  7.2 4.8 %copy-start.3 = (bf16[48,3,512]{2,0,1:T(8,128)(2,1)S(1)}, bf16[48,3,512]{2,0,1:T(8,128)(2,1)}, u32[]{:S(2)}) copy-start(bf16[48,3,512]{2,0,1:T(8,128)(2,1)} %param.19) | copy-start | bytes 442372
  7.2 4.8 %copy-start.7 = (f32[4,512]{1,0:T(4,128)S(1)}, f32[4,512]{1,0:T(4,128)}, u32[]{:S(2)}) copy-start(f32[4,512]{1,0:T(4,128)} %param.24) | copy-start | bytes 24580
  7.2 5.0 %copy-start.12 = (bf16[8,64,64]{2,1,0:T(8,128)(2,1)S(1)}, bf16[8,64,64]{2,1,0:T(8,128)(2,1)}, u32[]{:S(2)}) copy-start(bf16[8,64,64]{2,1,0:T(8,128)(2,1)} %param.25) | copy-start | bytes 196612
  7.2 46.3 %reduce-scatter.2.cloned.1.call-start = ((), (), s32[]{:S(2)}) async-start(), calls=%async_computation.3 | async-start | bytes 589824 | tf_op jit(solution)/shard_map/reduce_scatter | solution.py:106
  9.8 2.8 %copy-start.13 = (bf16[8,64,64]{2,1,0:T(8,128)(2,1)S(1)}, bf16[8,64,64]{2,1,0:T(8,128)(2,1)}, u32[]{:S(2)}) copy-start(bf16[8,64,64]{2,1,0:T(8,128)(2,1)} %param.26) | copy-start | bytes 196612
  12.0 1.0 %copy-start.9 = (f32[512]{0:T(512)S(1)}, f32[512]{0:T(512)}, u32[]{:S(2)}) copy-start(f32[512]{0:T(512)} %param.27) | copy-start | bytes 6148
  12.0 1.0 %copy-start.4 = (f32[48,512]{1,0:T(8,128)S(1)}, f32[48,512]{1,0:T(8,128)}, u32[]{:S(2)}) copy-start(f32[48,512]{1,0:T(8,128)} %param.20) | copy-start | bytes 294916
  12.1 1.1 %copy-start.5 = (f32[2048]{0:T(1024)S(1)}, f32[2048]{0:T(1024)}, u32[]{:S(2)}) copy-start(f32[2048]{0:T(1024)} %param.21) | copy-start | bytes 24580
  12.8 4.4 %copy-start.1 = (bf16[48,1024]{1,0:T(8,128)(2,1)S(1)}, bf16[48,1024]{1,0:T(8,128)(2,1)}, u32[]{:S(2)}) copy-start(bf16[48,1024]{1,0:T(8,128)(2,1)} %param.18) | copy-start | bytes 294916
  13.2 4.7 %copy-start.2 = (f32[48,512]{1,0:T(8,128)}, f32[48,512]{1,0:T(8,128)S(1)}, u32[]{:S(2)}) copy-start(f32[48,512]{1,0:T(8,128)S(1)} %multiply_add_fusion) | copy-start | bytes 294916
  13.2 7.2 %copy-start.6 = (s32[48,2]{0,1:T(2,128)S(1)}, s32[48,2]{0,1:T(2,128)}, u32[]{:S(2)}) copy-start(s32[48,2]{0,1:T(2,128)} %param.30) | copy-start | bytes 1156
  15.4 5.9 %copy-start.8 = (f32[2048]{0:T(1024)S(1)}, f32[2048]{0:T(1024)}, u32[]{:S(2)}) copy-start(f32[2048]{0:T(1024)} %param.29) | copy-start | bytes 24580
  43.7 3.9 %copy-start.10 = (f32[48,2]{0,1:T(2,128)S(1)}, f32[48,2]{0,1:T(2,128)}, u32[]{:S(2)}) copy-start(f32[48,2]{0,1:T(2,128)} %param.32) | copy-start | bytes 1156
  43.7 3.9 %copy-start.11 = (f32[48]{0:T(128)S(1)}, f32[48]{0:T(128)}, u32[]{:S(2)}) copy-start(f32[48]{0:T(128)} %param.31) | copy-start | bytes 580
  55.2 17.1 %all-to-all-start.1 = ((bf16[16,6,1024]{2,1,0:T(8,128)(2,1)}), bf16[16,6,1024]{2,1,0:T(8,128)(2,1)S(1)}, u32[]{:S(2)}, u32[]{:S(2)}) async-start(bf16[16,6,1024]{2,1,0:T(8,128)(2,1)} %copy.63), calls=%async_computation.2 | async-start | bytes 524288 | tf_op jit(solution)/shard_map/all_to_all | solution.py:109
Sparse Core Ops, SparseCore 0:
  47.7 5.7 reduce-scatter.1
where the time goes:
time: 82 us; the launch traced here: 81.5 us
  blocking collectives  27.2 us (33%)
  waiting for transfers between devices  15.8 us (19%)
  between operations  14.4 us (18%)
  matrix products  10.9 us (13%)
  starting transfers between devices  6.77 us (8%)
  local copies, waits for them, and re-layouts  4.27 us (5%)
  other arithmetic  2.18 us (3%)
    all_to_all x1, blocking collectives, local(): lax.all_to_all(outgoing, 'ep', split_axis=0, concat_axis=0, tiled=True)  18.2 us
    all_to_all x1, waiting for transfers between devices, local(): lax.all_to_all(summed, 'ep', split_axis=0, concat_axis=0, tiled=True)  9.95 us
    all_to_all x1, starting transfers between devices, local(): lax.all_to_all(summed, 'ep', split_axis=0, concat_axis=0, tiled=True)  6.73 us
    reduce_scatter x1, waiting for transfers between devices, local(): lax.psum_scatter(partial_value.astype(jnp.bfloat16), 'tp', scatter_dimens...  5.84 us
    psum x1, blocking collectives, local(): square_total = lax.psum(jnp.sum(values * values, axis=1), 'tp')  2.49 us
    all_gather x1, blocking collectives, local(): whole_tokens = lax.all_gather(tokens, 'tp', axis=1, tiled=True)  2.42 us
    dot_general x1, matrix products, local(): jnp.dot(hidden_units, expert_down[0], preferred_element_type=jnp.float32)  2.27 us
    dot_general x1, matrix products, local(): jnp.dot(normed, gelu_weight, preferred_element_type=jnp.float32)  2.18 us
  transfers between devices with their start and end apart: 2, of which 2 were waited for; matrix products, arithmetic and copies ran while one was open for 1% of the time, Pallas kernels for 0%

commit v1 on v0

--- a/solution.py
+++ b/solution.py
@@ -81,7 +81,7 @@
     )
     values = residual.astype(jnp.float32)
     half_width = values.shape[1]
-    square_total = lax.psum(jnp.sum(values * values, axis=1), "tp")
+    square_total = jnp.sum(lax.all_gather(jnp.sum(values * values, axis=1), "tp"), axis=0)
     gain_part = lax.dynamic_slice_in_dim(
         expert_gain, lax.axis_index("tp") * half_width, half_width, 0
     )

time: 82 us -> 83.6 us (1.020)
  local copies, waits for them, and re-layouts: 4.27 us -> 5.18 us
    psum x1 -> x0, blocking collectives: 2.49 us -> none  [local(): square_total = lax.psum(jnp.sum(values * values, axis=1), 'tp')]
    unnamed x0 -> x1, blocking collectives: none -> 2.46 us
where the time goes in v1:
time: 83.6 us; the launch traced here: 83.1 us
  blocking collectives  27.1 us (32%)
  waiting for transfers between devices  15.8 us (19%)
  between operations  15.1 us (18%)
  matrix products  10.9 us (13%)
  starting transfers between devices  6.77 us (8%)
  local copies, waits for them, and re-layouts  5.18 us (6%)
  other arithmetic  2.2 us (3%)
    all_to_all x1, blocking collectives, local(): lax.all_to_all(outgoing, 'ep', split_axis=0, concat_axis=0, tiled=True)  18.2 us
    all_to_all x1, waiting for transfers between devices, local(): lax.all_to_all(summed, 'ep', split_axis=0, concat_axis=0, tiled=True)  9.95 us
    all_to_all x1, starting transfers between devices, local(): lax.all_to_all(summed, 'ep', split_axis=0, concat_axis=0, tiled=True)  6.73 us
    reduce_scatter x1, waiting for transfers between devices, local(): lax.psum_scatter(partial_value.astype(jnp.bfloat16), 'tp', scatter_dimens...  5.84 us
    unnamed x1, blocking collectives  2.46 us
    all_gather x1, blocking collectives, local(): whole_tokens = lax.all_gather(tokens, 'tp', axis=1, tiled=True)  2.42 us
    dot_general x1, matrix products, local(): jnp.dot(hidden_units, expert_down[0], preferred_element_type=jnp.float32)  2.27 us
    dot_general x1, matrix products, local(): jnp.dot(normed, gelu_weight, preferred_element_type=jnp.float32)  2.18 us
  transfers between devices with their start and end apart: 2, of which 2 were waited for; matrix products, arithmetic and copies ran while one was open for 1% of the time, Pallas kernels for 0%

profile of v1, /device:TPU:0, one launch (start us, length us, event | category | flops | bytes accessed | tf_op | source)
XLA Modules:
  0.0 83.1 jit_solution(5435171774232731353)
XLA Ops:
  7.2 0.0 copy-start
  7.2 0.0 reduce-scatter.2.cloned.1.call-start
  7.3 2.4 %all_gather.15 = bf16[48,2048]{1,0:T(8,128)(2,1)S(1)} all-gather(bf16[48,1024]{1,0:T(8,128)(2,1)} %param.18), channel_id=1, replica_groups=mesh['ep'=16,'tp'=2] {'tp'}, dimensions={1}, use_global_device_ids=true | all-gather | bytes 294912 | tf_op jit(solution)/shard_map/all_gather | solution.py:35
  9.7 0.1 fusion.17
  9.9 2.2 %fusion.12 = bf16[48,1,512]{2,0,1:T(8,128)(2,1)S(1)} fusion(bf16[2048,512]{1,0:T(8,128)(2,1)} %param.22, bf16[48,2048]{1,0:T(8,128)(2,1)S(1)} %all_gather.15, f32[2048]{0:T(1024)} %param.21, f32[48]{0:T(128)S(1)} %add_rsqrt_fusion.1), kind=kOutput, calls=%fused_computation.21 | convolution fusion | flops 101081088 | bytes 2351296 | tf_op jit(solution)/shard_map/dot_general | solution.py:37
  12.0 0.0 copy-start.9
  12.1 0.0 copy-start.4
  12.1 0.0 copy-start.5
  12.1 0.1 convert_element_type.75
  12.3 0.2 fusion.7
  12.5 0.1 copy.55
  12.5 0.1 div.37
  12.6 0.2 fusion.3
  12.9 0.0 copy-start.1
  12.9 0.1 copy.57
  12.9 0.1 div.39
  13.1 0.0 copy-done.4
  13.1 0.1 multiply_add_fusion
  13.2 0.0 copy-start.2
  13.2 0.0 copy-start.14
  13.2 0.0 copy-start.6
  13.2 2.2 %fusion.28 = bf16[48,512]{1,0:T(8,128)(2,1)S(1)} fusion(f32[48,512]{1,0:T(8,128)S(1)} %multiply_add_fusion, bf16[2048,512]{1,0:T(8,128)(2,1)} %param.23, bf16[48,2048]{1,0:T(8,128)(2,1)S(1)} %all_gather.15, f32[2048]{0:T(1024)S(1)} %copy-done.5, f32[48]{0:T(128)S(1)} %add_rsqrt_fusion.1), kind=kOutput, calls=%fused_computation.46 | convolution fusion | flops 101351424 | bytes 2449600 | tf_op jit(solution)/shard_map/dot_general | solution.py:38
  15.4 0.0 copy-start.8
  15.4 1.9 %all_gather.16 = bf16[48,1024]{1,0:T(8,128)(2,1)S(1)} all-gather(bf16[48,512]{1,0:T(8,128)(2,1)S(1)} %fusion.28), channel_id=1, replica_groups=mesh['ep'=16,'tp'=2] {'tp'}, dimensions={1}, use_global_device_ids=true | all-gather | bytes 147456 | tf_op jit(solution)/shard_map/all_gather | solution.py:61
  17.3 0.0 copy-done
  17.3 0.6 multiply_reduce_fusion.2
  17.9 0.0 copy-done.2
  17.9 0.6 dynamic-slice
  19.2 0.2 dynamic-update-slice
  19.4 2.5 %all-reduce = f32[96]{0:T(128)S(1)} all-reduce(f32[96]{0:T(128)S(1)} %dynamic-update-slice), channel_id=2, replica_groups=mesh['ep'=16,'tp'=2] {'tp'}, use_global_device_ids=true, to_apply=%add | all-reduce | flops 96 | bytes 768
  21.9 0.1 reshape.127
  22.0 0.0 copy-done.6
  22.0 0.1 copy.59
  22.1 0.1 reshape.115
  22.2 0.1 fusion.36
  22.3 0.1 reduce_window_sum.11
  22.4 0.2 select_reduce_fusion
  22.6 0.1 reduce_sum.80
  22.7 0.1 copy.60
  22.8 0.1 convert_reduce_fusion
  23.0 0.3 convolution_convert_fusion.1
  23.2 0.1 reshape.116
  23.3 18.2 %all_to_all.10 = bf16[16,6,1024]{2,1,0:T(8,128)(2,1)S(1)} all-to-all(bf16[16,6,1024]{2,1,0:T(8,128)(2,1)S(1)} %reshape.116), channel_id=1, replica_groups=mesh['ep'=16,'tp'=2] {'ep'}, dimensions={0} | all-to-all | bytes 393216 | tf_op jit(solution)/shard_map/all_to_all | solution.py:93
  41.5 2.2 %all_gather.19 = bf16[16,6,2048]{2,1,0:T(8,128)(2,1)S(1)} all-gather(bf16[16,6,1024]{2,1,0:T(8,128)(2,1)S(1)} %all_to_all.10), channel_id=1, replica_groups=mesh['ep'=16,'tp'=2] {'tp'}, dimensions={2}, use_global_device_ids=true | all-gather | bytes 589824 | tf_op jit(solution)/shard_map/all_gather | solution.py:92
  43.7 0.1 reshape.117
  43.8 1.5 %fusion.15 = f32[96,256]{1,0:T(8,128)S(1)} fusion(bf16[96,2048]{1,0:T(8,128)(2,1)S(1)} %reshape.117, bf16[1,2048,256]{2,1,0:T(8,128)(2,1)} %param.33), kind=kOutput, calls=%fused_computation.24 | convolution fusion | flops 100663296 | bytes 1540096 | tf_op jit(solution)/shard_map/dot_general | solution.py:100
  45.3 0.0 copy-start.10
  45.3 0.0 copy-start.11
  45.4 1.5 %fusion.10 = bf16[96,256]{1,0:T(8,128)(2,1)S(1)} fusion(bf16[96,2048]{1,0:T(8,128)(2,1)S(1)} %reshape.117, bf16[1,2048,256]{2,1,0:T(8,128)(2,1)} %param.34, f32[96,256]{1,0:T(8,128)S(1)} %fusion.15), kind=kOutput, calls=%fused_computation.17 | convolution fusion | flops 100810752 | bytes 1589248 | tf_op jit(solution)/shard_map/dot_general | solution.py:101
  46.9 2.3 %convolution_convert_fusion = bf16[16,6,2048]{2,0,1:T(8,128)(2,1)} fusion(bf16[1,256,2048]{2,1,0:T(8,128)(2,1)} %param.35, bf16[16,6,256]{2,1,0:T(8,128)(2,1)S(1)} %dot_general.37), kind=kOutput, calls=%fused_computation.1 | convolution fusion | flops 100859904 | bytes 1490944 | tf_op jit(solution)/shard_map/dot_general | solution.py:103
  49.2 0.0 reduce-scatter.2.cloned.1.call-update
  49.3 5.8 %reduce-scatter.2.cloned.1.call-done = bf16[16,6,1024]{2,0,1:T(8,128)(2,1)} async-done(((bf16[16,6,2048]{2,0,1:T(8,128)(2,1)}), bf16[16,6,1024]{2,0,1:T(8,128)(2,1)}) %reduce-scatter.2.cloned.1.call-update) | async-done | bytes 196624 | tf_op jit(solution)/shard_map/reduce_scatter | solution.py:106
  55.1 1.7 %copy.63 = bf16[16,6,1024]{2,1,0:T(8,128)(2,1)} copy(bf16[16,6,1024]{2,0,1:T(8,128)(2,1)} %reduce-scatter.2.cloned.1.call-done) | data formatting | bytes 393216 | tf_op jit(solution)/shard_map/reduce_scatter | solution.py:106
  56.8 6.7 %all-to-all-start.1 = ((bf16[16,6,1024]{2,1,0:T(8,128)(2,1)}), bf16[16,6,1024]{2,1,0:T(8,128)(2,1)S(1)}, u32[]{:S(2)}, u32[]{:S(2)}) async-start(bf16[16,6,1024]{2,1,0:T(8,128)(2,1)} %copy.63), calls=%async_computation.2 | async-start | bytes 524288 | tf_op jit(solution)/shard_map/all_to_all | solution.py:109
  63.6 0.1 copy.64
  63.7 0.1 mul.189
  63.8 0.1 copy.61
  63.9 0.1 copy.58
  64.0 9.9 %all-to-all-done.1 = bf16[16,6,1024]{2,1,0:T(8,128)(2,1)S(1)} async-done(((bf16[16,6,1024]{2,1,0:T(8,128)(2,1)}), bf16[16,6,1024]{2,1,0:T(8,128)(2,1)S(1)}, u32[]{:S(2)}, u32[]{:S(2)}) %all-to-all-start.1) | async-done | bytes 196640 | tf_op jit(solution)/shard_map/all_to_all | solution.py:109
  74.0 0.1 reshape.118
  74.1 0.8 gather_fusion
  74.8 0.1 gather.7
  74.9 0.7 multiply_reduce_fusion
  75.6 0.7 add_convert_fusion
  (29 shorter events, 0.2 us)
Async XLA Ops:
  7.2 10.1 %copy-start = (bf16[1024,1024]{1,0:T(8,128)(2,1)S(1)}, bf16[1024,1024]{1,0:T(8,128)(2,1)}, u32[]{:S(2)}) copy-start(bf16[1024,1024]{1,0:T(8,128)(2,1)} %param.28) | copy-start | bytes 6291460
  7.2 4.8 %copy-start.3 = (bf16[48,3,512]{2,0,1:T(8,128)(2,1)S(1)}, bf16[48,3,512]{2,0,1:T(8,128)(2,1)}, u32[]{:S(2)}) copy-start(bf16[48,3,512]{2,0,1:T(8,128)(2,1)} %param.19) | copy-start | bytes 442372
  7.2 4.8 %copy-start.7 = (f32[4,512]{1,0:T(4,128)S(1)}, f32[4,512]{1,0:T(4,128)}, u32[]{:S(2)}) copy-start(f32[4,512]{1,0:T(4,128)} %param.24) | copy-start | bytes 24580
  7.2 5.0 %copy-start.12 = (bf16[8,64,64]{2,1,0:T(8,128)(2,1)S(1)}, bf16[8,64,64]{2,1,0:T(8,128)(2,1)}, u32[]{:S(2)}) copy-start(bf16[8,64,64]{2,1,0:T(8,128)(2,1)} %param.25) | copy-start | bytes 196612
  7.2 47.9 %reduce-scatter.2.cloned.1.call-start = ((), (), s32[]{:S(2)}) async-start(), calls=%async_computation.3 | async-start | bytes 589824 | tf_op jit(solution)/shard_map/reduce_scatter | solution.py:106
  9.8 2.8 %copy-start.13 = (bf16[8,64,64]{2,1,0:T(8,128)(2,1)S(1)}, bf16[8,64,64]{2,1,0:T(8,128)(2,1)}, u32[]{:S(2)}) copy-start(bf16[8,64,64]{2,1,0:T(8,128)(2,1)} %param.26) | copy-start | bytes 196612
  12.0 1.0 %copy-start.9 = (f32[512]{0:T(512)S(1)}, f32[512]{0:T(512)}, u32[]{:S(2)}) copy-start(f32[512]{0:T(512)} %param.27) | copy-start | bytes 6148
  12.1 1.0 %copy-start.4 = (f32[48,512]{1,0:T(8,128)S(1)}, f32[48,512]{1,0:T(8,128)}, u32[]{:S(2)}) copy-start(f32[48,512]{1,0:T(8,128)} %param.20) | copy-start | bytes 294916
  12.1 1.1 %copy-start.5 = (f32[2048]{0:T(1024)S(1)}, f32[2048]{0:T(1024)}, u32[]{:S(2)}) copy-start(f32[2048]{0:T(1024)} %param.21) | copy-start | bytes 24580
  12.9 4.5 %copy-start.1 = (bf16[48,1024]{1,0:T(8,128)(2,1)S(1)}, bf16[48,1024]{1,0:T(8,128)(2,1)}, u32[]{:S(2)}) copy-start(bf16[48,1024]{1,0:T(8,128)(2,1)} %param.18) | copy-start | bytes 294916
  13.2 4.7 %copy-start.2 = (f32[48,512]{1,0:T(8,128)}, f32[48,512]{1,0:T(8,128)S(1)}, u32[]{:S(2)}) copy-start(f32[48,512]{1,0:T(8,128)S(1)} %multiply_add_fusion) | copy-start | bytes 294916
  13.2 4.7 %copy-start.14 = (u32[32]{0:T(128)S(1)}, u32[32]{0:T(128)}, u32[]{:S(2)}) copy-start(u32[32]{0:T(128)} %constant.60) | copy-start | bytes 388
  13.2 8.8 %copy-start.6 = (s32[48,2]{0,1:T(2,128)S(1)}, s32[48,2]{0,1:T(2,128)}, u32[]{:S(2)}) copy-start(s32[48,2]{0,1:T(2,128)} %param.30) | copy-start | bytes 1156
  15.4 7.5 %copy-start.8 = (f32[2048]{0:T(1024)S(1)}, f32[2048]{0:T(1024)}, u32[]{:S(2)}) copy-start(f32[2048]{0:T(1024)} %param.29) | copy-start | bytes 24580
  45.3 3.9 %copy-start.10 = (f32[48,2]{0,1:T(2,128)S(1)}, f32[48,2]{0,1:T(2,128)}, u32[]{:S(2)}) copy-start(f32[48,2]{0,1:T(2,128)} %param.32) | copy-start | bytes 1156
  45.3 3.9 %copy-start.11 = (f32[48]{0:T(128)S(1)}, f32[48]{0:T(128)}, u32[]{:S(2)}) copy-start(f32[48]{0:T(128)} %param.31) | copy-start | bytes 580
  56.8 17.1 %all-to-all-start.1 = ((bf16[16,6,1024]{2,1,0:T(8,128)(2,1)}), bf16[16,6,1024]{2,1,0:T(8,128)(2,1)S(1)}, u32[]{:S(2)}, u32[]{:S(2)}) async-start(bf16[16,6,1024]{2,1,0:T(8,128)(2,1)} %copy.63), calls=%async_computation.2 | async-start | bytes 524288 | tf_op jit(solution)/shard_map/all_to_all | solution.py:109
Sparse Core Ops, SparseCore 0:
  49.3 5.7 reduce-scatter.1
